TPU v7x, 512 devices: a 8x2x16 block of a 8x16x16 slice. The times are simulated.
512 devices in a mesh: grp: 2 (over y), kv: 16 (over z), tp: 16 (over x, core).
Axes of the slice: x: 8, y: 2, z: 16, core: 2. Of those that a mesh axis runs over, the one named last changes fastest.
The devices are a block of a 8x16x16 slice.
Arguments:
- tokens: bfloat16 [640, 4096], P('grp', ('kv', 'tp')), parts along dimension 0, may hold values from -65 to 65
- lengths: int32 [640], P(('grp', 'kv')), parts along dimension 0, may hold values from 1 to 16384, 1310720 in all
- memory: float32 [640, 16, 128, 128], P(('grp', 'kv'), 'tp'), parts along dimension 0, may hold values from -6 to 6
- norm_attn: bfloat16 [4096], P('kv'), may hold values from 0.099609375 to 1.8984375
- w_query: bfloat16 [4096, 2048], P('kv', 'tp'), may hold values from -0.09375 to 0.09375
- w_key: bfloat16 [4096, 2048], P('kv', 'tp'), may hold values from -0.09375 to 0.09375
- w_value: bfloat16 [4096, 2048], P('kv', 'tp'), may hold values from -0.09375 to 0.09375
- w_gate: bfloat16 [4096, 2048], P('kv', 'tp'), may hold values from -0.09375 to 0.09375
- head_gain: bfloat16 [2048], P('tp'), may hold values from 0.099609375 to 1.8984375
- w_out: bfloat16 [2048, 4096], P('tp', 'kv'), may hold values from -0.1875 to 0.1875
- norm_mlp: bfloat16 [4096], P('kv'), may hold values from 0.099609375 to 1.8984375
- w_gate_mlp: bfloat16 [4096, 14336], P('kv', 'tp'), may hold values from -0.09375 to 0.09375
- w_up: bfloat16 [4096, 14336], P('kv', 'tp'), may hold values from -0.09375 to 0.09375
- w_down: bfloat16 [14336, 4096], P('tp', 'kv'), may hold values from -0.0625 to 0.0625
Outputs:
- result: bfloat16 [640, 4096], P('grp', ('kv', 'tp')), parts along dimension 0
- new_memory: float32 [640, 16, 128, 128], P(('grp', 'kv'), 'tp'), parts along dimension 0
There are 2 independent parts, one for each index of `grp`. A program takes and returns all parts, laid end to end along the dimension named above; an argument that names none is the same for every part. Nothing has to cross between parts.
Inputs may be any that keep to these rules, and one draw needn't show every extreme that they name: Within each part along grp the lengths sum to 1310720 and the longest is exactly 16384.
All inputs are finite; a program needn't handle non-finite values. No bound on the sum of `lengths` on one device may be relied on, other than what follows from the above.
Results may differ from a plain program's by a relative error of at most 0.025.
Values may be sent and summed in bfloat16 or wider, within the bound.
No kernel may reach another device: no remote copies, remote signals or barrier semaphores. Data moves between devices by JAX's collectives and lax.ppermute only.
A program may use at most 64 MiB of HBM per device.

v0:
```python
import jax
import jax.numpy as jnp
from jax import lax
from jax.sharding import PartitionSpec as P

D = 4096
HEADS = 16
epsilon = 1e-06


def from_everyone(array, axis):
    copies = jnp.broadcast_to(array, (lax.axis_size(axis), *array.shape))
    return lax.all_to_all(copies, axis, split_axis=0, concat_axis=0, tiled=True)


def taken_together(array, axis):
    everything = from_everyone(array, axis)
    return jnp.sum(everything, axis=0)


def in_blocks(array, dim, size):
    lengths = array.shape
    pieces = array.reshape(*lengths[:dim], size, lengths[dim] // size, *lengths[dim + 1 :])
    return jnp.moveaxis(pieces, dim, 0)


def sum_at_owner(array, axis, dim):
    size = lax.axis_size(axis)
    pieces = lax.all_to_all(in_blocks(array, dim, size), axis, 0, 0, tiled=True)
    return jnp.sum(pieces.astype(jnp.float32), axis=0)


def rotate(values, position):
    half_width = values.shape[-1] // 2
    inverse = 10000.0 ** (-jnp.arange(half_width, dtype=jnp.float32) / half_width)
    angles = position[:, None] * inverse[None, :]
    cosine = jnp.cos(angles)[:, None, :]
    sine = jnp.sin(angles)[:, None, :]
    first = values[..., :half_width]
    second = values[..., half_width:]
    return jnp.concatenate(
        [first * cosine - second * sine, second * cosine + first * sine], axis=-1
    )


def head_decay(head_index):
    exponent = -5.0 - head_index.astype(jnp.float32) * (7.0 / max(HEADS - 1, 1))
    return 1.0 - jnp.exp2(exponent)


def retain(memory, queries, key_rows, value_rows, gate_rows, head_gain, decay_rate):
    new_memory = (
        decay_rate[None, :, None, None] * memory
        + key_rows[:, :, :, None] * value_rows[:, :, None, :]
    )
    readout = jnp.einsum(
        "bhd,bhde->bhe",
        queries * queries.shape[-1] ** (-0.5),
        new_memory,
        precision=lax.Precision.HIGHEST,
    )
    centred = readout - jnp.mean(readout, axis=-1, keepdims=True)
    normed = centred * lax.rsqrt(jnp.mean(centred * centred, axis=-1, keepdims=True) + epsilon)
    normed = normed.reshape(readout.shape[0], -1) * head_gain.astype(jnp.float32)
    return (new_memory, (normed * jax.nn.silu(gate_rows)).astype(jnp.bfloat16))


def per_device(
    tokens,
    lengths,
    memory,
    norm_attn,
    w_query,
    w_key,
    w_value,
    w_gate,
    head_gain,
    w_out,
    norm_mlp,
    w_gate_mlp,
    w_up,
    w_down,
):
    own_count = memory.shape[0]
    heads_local = memory.shape[1]
    head_size = memory.shape[2]
    width_local = w_query.shape[1]
    gathered = lax.all_gather(tokens, "tp", axis=1, tiled=True)
    tok_float = gathered.astype(jnp.float32)
    square_part = jnp.sum(tok_float * tok_float, axis=1)
    scaled = (tok_float * norm_attn.astype(jnp.float32)).astype(jnp.bfloat16)
    own_start = lax.axis_index("kv") * own_count
    square_total = taken_together(square_part, "kv")
    own_squares = lax.dynamic_slice_in_dim(square_total, own_start, own_count, 0)
    block_rows = scaled
    projected = sum_at_owner(
        jnp.concatenate(
            [
                jnp.dot(block_rows, weight, preferred_element_type=jnp.float32)
                for weight in (w_query, w_key, w_value, w_gate)
            ],
            axis=1,
        ).astype(jnp.bfloat16),
        "kv",
        0,
    )
    projected = projected * lax.rsqrt(own_squares / D + epsilon)[:, None]
    position = lengths.astype(jnp.float32)
    queries = rotate(
        projected[:, :width_local].reshape(own_count, heads_local, head_size), position
    )
    key_rows = rotate(
        projected[:, width_local : 2 * width_local].reshape(own_count, heads_local, head_size),
        position,
    )
    value_rows = projected[:, 2 * width_local : 3 * width_local].reshape(
        own_count, heads_local, head_size
    )
    gate_rows = projected[:, 3 * width_local :]
    decay_rate = head_decay(lax.axis_index("tp") * heads_local + jnp.arange(heads_local))
    new_memory, mixed = retain(
        memory, queries, key_rows, value_rows, gate_rows, head_gain, decay_rate
    )
    attn_part = jnp.dot(
        lax.all_gather(mixed, "kv", axis=0, tiled=True), w_out, preferred_element_type=jnp.float32
    )
    attn_total = sum_at_owner(attn_part.astype(jnp.bfloat16), "tp", 1)
    middle = (tokens.astype(jnp.float32) + attn_total).astype(jnp.bfloat16)
    mid_float = middle.astype(jnp.float32)
    gathered_mid = lax.all_gather(middle, "tp", axis=1, tiled=True)
    gathered_float = gathered_mid.astype(jnp.float32)
    mid_squares = jnp.sum(gathered_float * gathered_float, axis=1)
    scaled_mid = (gathered_float * norm_mlp.astype(jnp.float32)).astype(jnp.bfloat16)
    ff_local = w_up.shape[1]
    pieces = 1
    span = scaled_mid.shape[0] // pieces
    own_span = span // lax.axis_size("kv")
    span_start = lax.axis_index("kv") * own_span
    square_sums = taken_together(mid_squares, "kv")
    span_squares = lax.dynamic_slice_in_dim(square_sums, span_start, own_span, 0)
    block_rows = scaled_mid
    both_terms = lax.psum_scatter(
        jnp.concatenate(
            [
                jnp.dot(block_rows, w_gate_mlp, preferred_element_type=jnp.float32),
                jnp.dot(block_rows, w_up, preferred_element_type=jnp.float32),
            ],
            axis=1,
        ).astype(jnp.bfloat16),
        "kv",
        scatter_dimension=0,
        tiled=True,
    ).astype(jnp.float32)
    inv_mlp = lax.rsqrt(span_squares / D + epsilon)[:, None]
    gate_mlp = inv_mlp * both_terms[:, :ff_local]
    up_rows = inv_mlp * both_terms[:, ff_local:]
    hidden = (jax.nn.silu(gate_mlp) * up_rows).astype(jnp.bfloat16)
    partial_mlp = jnp.dot(
        lax.all_gather(hidden, "kv", axis=0, tiled=True), w_down, preferred_element_type=jnp.float32
    )
    results = sum_at_owner(partial_mlp.astype(jnp.bfloat16), "tp", 1)
    return ((mid_float + results).astype(jnp.bfloat16), new_memory)


def solution(mesh):
    in_specs = (
        P("grp", ("kv", "tp")),
        P(("grp", "kv")),
        P(("grp", "kv"), "tp", None, None),
        P("kv"),
        P("kv", "tp"),
        P("kv", "tp"),
        P("kv", "tp"),
        P("kv", "tp"),
        P("tp"),
        P("tp", "kv"),
        P("kv"),
        P("kv", "tp"),
        P("kv", "tp"),
        P("tp", "kv"),
    )
    out_specs = (P("grp", ("kv", "tp")), P(("grp", "kv"), "tp", None, None))
    return jax.shard_map(
        per_device, mesh=mesh, in_specs=in_specs, out_specs=out_specs, check_vma=False
    )
```

profile of v0, /device:TPU:65, one launch (start us, length us, event | category | flops | bytes accessed | tf_op | source)
XLA Modules:
  0.0 281.9 jit_solution(7506747860716999850)
XLA Ops:
  0.6 0.0 copy-start
  0.7 56.5 %all_gather.12 = bf16[320,256]{0,1:T(8,128)(2,1)S(1)} all-gather(bf16[320,16]{0,1:T(8,128)(2,1)} %param.14), channel_id=1, replica_groups=mesh['grp'=2,'kv'=16,'tp'=16] {'tp'}, dimensions={1}, use_global_device_ids=true | all-gather | bytes 174080 | tf_op jit(solution)/shard_map/all_gather | solution.py:88
  57.1 0.1 fusion.4
  57.2 0.6 broadcast_in_dim.4
  57.8 7.1 %all-to-all-start.1 = ((f32[16,1,320]{2,1,0:T(1,128)}), f32[16,1,320]{2,1,0:T(1,128)S(1)}, u32[]{:S(2)}, u32[]{:S(2)}) async-start(f32[16,1,320]{2,1,0:T(1,128)} %broadcast_in_dim.4), calls=%async_computation.1 | async-start | bytes 49152 | tf_op jit(solution)/shard_map/all_to_all | solution.py:13
  64.9 0.7 convert_element_type.69
  65.6 1.1 convolution_convert_fusion.6
  66.8 1.2 convolution_convert_fusion.5
  68.0 0.0 copy-start.9
  68.0 0.0 copy-start.10
  68.0 0.3 convolution_convert_fusion.4
  68.3 0.3 convolution_convert_fusion.7
  68.7 0.0 copy-start.2
  68.7 0.8 pad_maximum_fusion.1
  69.5 6.7 %all-to-all-done.1 = f32[16,1,320]{2,1,0:T(1,128)S(1)} async-done(((f32[16,1,320]{2,1,0:T(1,128)}), f32[16,1,320]{2,1,0:T(1,128)S(1)}, u32[]{:S(2)}, u32[]{:S(2)}) %all-to-all-start.1) | async-done | bytes 20512 | tf_op jit(solution)/shard_map/all_to_all | solution.py:13
  76.2 4.7 %all-to-all-start = ((bf16[16,20,512]{2,1,0:T(8,128)(2,1)}), bf16[16,20,512]{2,1,0:T(8,128)(2,1)S(1)}, u32[]{:S(2)}, u32[]{:S(2)}) async-start(bf16[16,20,512]{2,1,0:T(8,128)(2,1)} %pad_maximum_fusion.1), calls=%async_computation | async-start | bytes 786432 | tf_op jit(solution)/shard_map/all_to_all | solution.py:29
  81.1 0.1 add_rsqrt_fusion.2
  81.2 17.7 %all-to-all-done = bf16[16,20,512]{2,1,0:T(8,128)(2,1)S(1)} async-done(((bf16[16,20,512]{2,1,0:T(8,128)(2,1)}), bf16[16,20,512]{2,1,0:T(8,128)(2,1)S(1)}, u32[]{:S(2)}, u32[]{:S(2)}) %all-to-all-start) | async-done | bytes 327712 | tf_op jit(solution)/shard_map/all_to_all | solution.py:29
  98.9 0.1 convert_reduce_fusion
  99.0 0.1 broadcast_multiply_fusion
  99.0 0.1 fusion.21
  99.2 0.1 fusion.26
  99.3 0.1 maximum_bitcast_fusion
  99.3 0.4 multiply_add_fusion
  99.8 0.0 copy-start.1
  99.8 0.0 copy-start.5
  99.8 0.0 copy-start.11
  99.8 0.0 copy-start.8
  99.8 1.2 fusion.1
  101.0 0.1 bitcast_reduce_fusion
  101.1 0.2 multiply_reduce_fusion
  101.3 0.1 fusion.28
  101.4 26.0 %all-gather = bf16[16,20,128]{2,1,0:T(8,128)(2,1)S(1)} all-gather(bf16[1,20,128]{2,1,0:T(8,128)(2,1)S(1)} %fusion.28), channel_id=1, replica_groups=mesh['grp'=2,'kv'=16,'tp'=16] {'kv'}, dimensions={0}, use_global_device_ids=true | all-gather | bytes 87040 | tf_op jit(solution)/shard_map/all_gather | solution.py:125
  127.4 0.2 convolution_convert_fusion.3
  127.6 0.0 copy-start.3
  127.6 0.8 copy.23
  128.4 15.3 %all-to-all-start.2 = ((bf16[16,320,16]{1,2,0:T(8,128)(2,1)}), bf16[16,320,16]{1,2,0:T(8,128)(2,1)S(1)}, u32[]{:S(2)}, u32[]{:S(2)}) async-start(bf16[16,320,16]{1,2,0:T(8,128)(2,1)} %bitcast.10), calls=%async_computation.2 | async-start | bytes 393216 | tf_op jit(solution)/shard_map/all_to_all | solution.py:29
  143.7 1.3 dynamic-slice.4
  145.7 8.3 %all-to-all-done.2 = bf16[16,320,16]{1,2,0:T(8,128)(2,1)S(1)} async-done(((bf16[16,320,16]{1,2,0:T(8,128)(2,1)}), bf16[16,320,16]{1,2,0:T(8,128)(2,1)S(1)}, u32[]{:S(2)}, u32[]{:S(2)}) %all-to-all-start.2) | async-done | bytes 163872 | tf_op jit(solution)/shard_map/all_to_all | solution.py:29
  154.0 15.1 %all_gather.14 = bf16[320,256]{0,1:T(8,128)(2,1)S(1)} all-gather(bf16[320,16]{0,1:T(8,128)(2,1)S(1)} %add_convert_fusion.1), channel_id=1, replica_groups=mesh['grp'=2,'kv'=16,'tp'=16] {'tp'}, dimensions={1}, use_global_device_ids=true | all-gather | bytes 174080 | tf_op jit(solution)/shard_map/all_gather | solution.py:130
  169.1 0.1 fusion.5
  169.1 0.6 broadcast_in_dim.5
  169.8 4.7 %all-to-all-start.3 = ((f32[16,1,320]{2,1,0:T(1,128)}), f32[16,1,320]{2,1,0:T(1,128)S(1)}, u32[]{:S(2)}, u32[]{:S(2)}) async-start(f32[16,1,320]{2,1,0:T(1,128)} %broadcast_in_dim.5), calls=%async_computation.3 | async-start | bytes 49152 | tf_op jit(solution)/shard_map/all_to_all | solution.py:13
  174.4 0.4 convolution_convert_fusion
  174.9 0.4 convolution_convert_fusion.1
  175.3 0.1 pad_maximum_fusion
  175.4 32.2 %fusion = bf16[24,1792]{1,0:T(8,128)(2,1)S(1)} fusion(bf16[320,1792]{1,0:T(8,128)(2,1)S(1)} %pad_maximum_fusion), kind=kCustom, calls=%all-reduce-scatter | all-reduce-scatter fusion | flops 688129 | bytes 1234944
  207.6 2.7 collective-permute-start.1
  210.3 2.9 %collective-permute-start = (bf16[24,1792]{1,0:T(8,128)(2,1)S(1)}, bf16[24,1792]{1,0:T(8,128)(2,1)S(1)}, u32[]{:S(2)}, u32[]{:S(2)}) collective-permute-start(bf16[24,1792]{1,0:T(8,128)(2,1)S(1)} %fusion), channel_id=1, source_target_pairs={{0,16},{16,32},{32,48},{48,64},{64,80},{80,96},{96,112},{112,128},... | collective-permute-start | bytes 258056
  213.3 5.5 %collective-permute-start.2 = (bf16[12,1792]{1,0:T(8,128)(2,1)S(1)}, bf16[12,1792]{1,0:T(8,128)(2,1)S(1)}, u32[]{:S(2)}, u32[]{:S(2)}) collective-permute-start(bf16[12,1792]{1,0:T(8,128)(2,1)S(1)} %slice.50), channel_id=1, source_target_pairs={{0,48},{16,64},{32,80},{48,96},{64,112},{80,128},{96,144},{112,160... | collective-permute-start | bytes 129032
  218.8 0.0 all-to-all-done.3
  218.9 0.1 add_rsqrt_fusion
  218.9 1.1 collective-permute-done.2
  220.0 0.0 collective-permute-done.1
  220.0 0.0 collective-permute-done
  220.1 0.6 concatenate.40
  220.6 0.0 copy-start.4
  220.7 0.1 fusion.11
  220.8 28.5 %all-gather.1 = bf16[16,20,896]{2,1,0:T(8,128)(2,1)S(1)} all-gather(bf16[1,20,896]{2,1,0:T(8,128)(2,1)S(1)} %fusion.11), channel_id=1, replica_groups=mesh['grp'=2,'kv'=16,'tp'=16] {'kv'}, dimensions={0}, use_global_device_ids=true | all-gather | bytes 609280 | tf_op jit(solution)/shard_map/all_gather | solution.py:159
  249.3 0.1 reshape.198
  249.5 0.3 convolution_convert_fusion.2
  249.8 0.2 copy.25
  250.0 31.3 %all_to_all.27 = bf16[16,320,16]{1,2,0:T(8,128)(2,1)S(1)} all-to-all(bf16[16,320,16]{1,2,0:T(8,128)(2,1)S(1)} %bitcast.47), channel_id=1, replica_groups=mesh['grp'=2,'kv'=16,'tp'=16] {'tp'}, dimensions={0} | all-to-all | bytes 327680 | tf_op jit(solution)/shard_map/all_to_all | solution.py:29
  281.3 0.6 add_convert_fusion
  (33 shorter events, 0.4 us)
Async XLA Ops:
  0.6 173.8 %copy-start = (bf16[256,896]{1,0:T(8,128)(2,1)S(1)}, bf16[256,896]{1,0:T(8,128)(2,1)}, u32[]{:S(2)}) copy-start(bf16[256,896]{1,0:T(8,128)(2,1)} %param.26) | copy-start | bytes 1376260
  0.6 67.3 %copy-start.6 = (bf16[256,128]{1,0:T(8,128)(2,1)S(1)}, bf16[256,128]{1,0:T(8,128)(2,1)}, u32[]{:S(2)}) copy-start(bf16[256,128]{1,0:T(8,128)(2,1)} %param.21) | copy-start | bytes 196612
  0.7 67.7 %copy-start.7 = (bf16[256,128]{1,0:T(8,128)(2,1)S(1)}, bf16[256,128]{1,0:T(8,128)(2,1)}, u32[]{:S(2)}) copy-start(bf16[256,128]{1,0:T(8,128)(2,1)} %param.18) | copy-start | bytes 196612
  57.8 18.4 %all-to-all-start.1 = ((f32[16,1,320]{2,1,0:T(1,128)}), f32[16,1,320]{2,1,0:T(1,128)S(1)}, u32[]{:S(2)}, u32[]{:S(2)}) async-start(f32[16,1,320]{2,1,0:T(1,128)} %broadcast_in_dim.4), calls=%async_computation.1 | async-start | bytes 49152 | tf_op jit(solution)/shard_map/all_to_all | solution.py:13
  68.0 13.1 %copy-start.9 = (s32[20]{0:T(128)S(1)}, s32[20]{0:T(128)}, u32[]{:S(2)}) copy-start(s32[20]{0:T(128)} %param.15) | copy-start | bytes 244
  68.0 13.1 %copy-start.10 = (bf16[128]{0:T(256)(128)(2,1)S(1)}, bf16[128]{0:T(256)(128)(2,1)}, u32[]{:S(2)}) copy-start(bf16[128]{0:T(256)(128)(2,1)} %param.22) | copy-start | bytes 772
  68.7 30.7 %copy-start.2 = (f32[20,1,128,128]{3,2,1,0:T(8,128)S(1)}, f32[20,1,128,128]{3,2,1,0:T(8,128)}, u32[]{:S(2)}) copy-start(f32[20,1,128,128]{3,2,1,0:T(8,128)} %param.16) | copy-start | bytes 3932164
  76.2 22.7 %all-to-all-start = ((bf16[16,20,512]{2,1,0:T(8,128)(2,1)}), bf16[16,20,512]{2,1,0:T(8,128)(2,1)S(1)}, u32[]{:S(2)}, u32[]{:S(2)}) async-start(bf16[16,20,512]{2,1,0:T(8,128)(2,1)} %pad_maximum_fusion.1), calls=%async_computation | async-start | bytes 786432 | tf_op jit(solution)/shard_map/all_to_all | solution.py:29
  99.8 28.7 %copy-start.1 = (f32[20,1,128,128]{3,2,1,0:T(8,128)}, f32[20,1,128,128]{3,2,1,0:T(8,128)S(1)}, u32[]{:S(2)}) copy-start(f32[20,1,128,128]{3,2,1,0:T(8,128)S(1)} %multiply_add_fusion) | copy-start | bytes 3932164
  99.8 27.6 %copy-start.5 = (bf16[128,256]{1,0:T(8,128)(2,1)S(1)}, bf16[128,256]{1,0:T(8,128)(2,1)}, u32[]{:S(2)}) copy-start(bf16[128,256]{1,0:T(8,128)(2,1)} %param.23) | copy-start | bytes 196612
  99.8 43.9 %copy-start.11 = (bf16[256]{0:T(256)(128)(2,1)S(1)}, bf16[256]{0:T(256)(128)(2,1)}, u32[]{:S(2)}) copy-start(bf16[256]{0:T(256)(128)(2,1)} %param.24) | copy-start | bytes 1540
  99.8 54.2 %copy-start.8 = (bf16[320,16]{0,1:T(8,128)(2,1)S(1)}, bf16[320,16]{0,1:T(8,128)(2,1)}, u32[]{:S(2)}) copy-start(bf16[320,16]{0,1:T(8,128)(2,1)} %param.14) | copy-start | bytes 30724
  127.6 47.3 %copy-start.3 = (bf16[256,896]{1,0:T(8,128)(2,1)S(1)}, bf16[256,896]{1,0:T(8,128)(2,1)}, u32[]{:S(2)}) copy-start(bf16[256,896]{1,0:T(8,128)(2,1)} %param.25) | copy-start | bytes 1376260
  128.4 25.5 %all-to-all-start.2 = ((bf16[16,320,16]{1,2,0:T(8,128)(2,1)}), bf16[16,320,16]{1,2,0:T(8,128)(2,1)S(1)}, u32[]{:S(2)}, u32[]{:S(2)}) async-start(bf16[16,320,16]{1,2,0:T(8,128)(2,1)} %bitcast.10), calls=%async_computation.2 | async-start | bytes 393216 | tf_op jit(solution)/shard_map/all_to_all | solution.py:29
  169.8 49.1 %all-to-all-start.3 = ((f32[16,1,320]{2,1,0:T(1,128)}), f32[16,1,320]{2,1,0:T(1,128)S(1)}, u32[]{:S(2)}, u32[]{:S(2)}) async-start(f32[16,1,320]{2,1,0:T(1,128)} %broadcast_in_dim.5), calls=%async_computation.3 | async-start | bytes 49152 | tf_op jit(solution)/shard_map/all_to_all | solution.py:13
  207.6 12.4 %collective-permute-start.1 = (bf16[24,1792]{1,0:T(8,128)(2,1)S(1)}, bf16[24,1792]{1,0:T(8,128)(2,1)S(1)}, u32[]{:S(2)}, u32[]{:S(2)}) collective-permute-start(bf16[24,1792]{1,0:T(8,128)(2,1)S(1)} %fusion), channel_id=1, source_target_pairs={{0,32},{16,48},{32,64},{48,80},{64,96},{80,112},{96,128},{112,144}... | collective-permute-start | bytes 258056
  210.3 9.7 %collective-permute-start = (bf16[24,1792]{1,0:T(8,128)(2,1)S(1)}, bf16[24,1792]{1,0:T(8,128)(2,1)S(1)}, u32[]{:S(2)}, u32[]{:S(2)}) collective-permute-start(bf16[24,1792]{1,0:T(8,128)(2,1)S(1)} %fusion), channel_id=1, source_target_pairs={{0,16},{16,32},{32,48},{48,64},{64,80},{80,96},{96,112},{112,128},... | collective-permute-start | bytes 258056
  213.3 6.8 %collective-permute-start.2 = (bf16[12,1792]{1,0:T(8,128)(2,1)S(1)}, bf16[12,1792]{1,0:T(8,128)(2,1)S(1)}, u32[]{:S(2)}, u32[]{:S(2)}) collective-permute-start(bf16[12,1792]{1,0:T(8,128)(2,1)S(1)} %slice.50), channel_id=1, source_target_pairs={{0,48},{16,64},{32,80},{48,96},{64,112},{80,128},{96,144},{112,160... | collective-permute-start | bytes 129032
  220.6 28.8 %copy-start.4 = (bf16[896,256]{1,0:T(8,128)(2,1)S(1)}, bf16[896,256]{1,0:T(8,128)(2,1)}, u32[]{:S(2)}) copy-start(bf16[896,256]{1,0:T(8,128)(2,1)} %param.27) | copy-start | bytes 1376260
where the time goes:
time: 283 us; the launch traced here: 282 us
  blocking collectives  190 us (67%)
  starting transfers between devices  42.9 us (15%)
  waiting for transfers between devices  33.8 us (12%)
  matrix products  5.51 us (2%)
  local copies, waits for them, and re-layouts  4.37 us (2%)
  other arithmetic  4 us (1%)
    all_gather x1, blocking collectives, per_device(): gathered = lax.all_gather(tokens, 'tp', axis=1, tiled=True)  56.5 us
    unnamed x1, blocking collectives  32.2 us
    all_to_all x1, blocking collectives, sum_at_owner(): pieces = lax.all_to_all(in_blocks(array, dim, size), axis, 0, 0, tiled=True)  31.3 us
    all_gather x1, blocking collectives, per_device(): lax.all_gather(hidden, 'kv', axis=0, tiled=True)  28.5 us
    all_gather x1, blocking collectives, per_device(): lax.all_gather(mixed, 'kv', axis=0, tiled=True)  26 us
    all_to_all x2, waiting for transfers between devices, sum_at_owner(): pieces = lax.all_to_all(in_blocks(array, dim, size), axis, 0, 0, tiled=True)  25.9 us
    all_to_all x2, starting transfers between devices, sum_at_owner(): pieces = lax.all_to_all(in_blocks(array, dim, size), axis, 0, 0, tiled=True)  20 us
    all_gather x1, blocking collectives, per_device(): gathered_mid = lax.all_gather(middle, 'tp', axis=1, tiled=True)  15.1 us
  transfers between devices with their start and end apart: 7, of which 4 were waited for; matrix products, arithmetic and copies ran while one was open for 14% of the time, Pallas kernels for 0%

commit v1 on v0

--- a/solution.py
+++ b/solution.py
@@ -6,6 +6,28 @@
 D = 4096
 HEADS = 16
 epsilon = 1e-06
+
+
+def joined_along(blocks, dim):
+    blocks = jnp.moveaxis(blocks, 0, dim)
+    shape = blocks.shape
+    return blocks.reshape(*shape[:dim], shape[dim] * shape[dim + 1], *shape[dim + 2 :])
+
+
+def ring_gather(x, axis, dim):
+    size = lax.axis_size(axis)
+    pairs = [(i, (i + 1) % size) for i in range(size)]
+    back = [(b, a) for a, b in pairs]
+    lower, upper = ([], [])
+    for step in range(size - 1):
+        if step % 2 == 0:
+            lower.append(lax.ppermute(lower[-1] if lower else x, axis, pairs))
+        else:
+            upper.append(lax.ppermute(upper[-1] if upper else x, axis, back))
+    blocks = jnp.stack([*lower[::-1], x, *upper])
+    shift = lax.axis_index(axis) - len(lower)
+    blocks = blocks[(jnp.arange(size) - shift) % size]
+    return joined_along(blocks, dim)
 
 
 def from_everyone(array, axis):
@@ -85,7 +107,7 @@
     heads_local = memory.shape[1]
     head_size = memory.shape[2]
     width_local = w_query.shape[1]
-    gathered = lax.all_gather(tokens, "tp", axis=1, tiled=True)
+    gathered = ring_gather(tokens, "tp", 1)
     tok_float = gathered.astype(jnp.float32)
     square_part = jnp.sum(tok_float * tok_float, axis=1)
     scaled = (tok_float * norm_attn.astype(jnp.float32)).astype(jnp.bfloat16)

time: 283 us -> 301 us (1.064)
  blocking collectives: 190 us -> 133 us
  waiting for transfers between devices: 33.8 us -> 74.8 us
  starting transfers between devices: 42.9 us -> 75.1 us
  local copies, waits for them, and re-layouts: 4.37 us -> 8.23 us
    all_gather x1 -> x0, blocking collectives: 56.5 us -> none  [per_device(): gathered = lax.all_gather(tokens, 'tp', axis=1, tiled=True)]
    ppermute x0 -> x15, waiting for transfers between devices: none -> 44.5 us  [the longest x8 42.5 us: ring_gather(): lower.append(lax.ppermute(lower[-1] if lower else x, axis, pairs))]
    ppermute x0 -> x15, starting transfers between devices: none -> 27.5 us  [the longest x7 24.8 us: ring_gather(): upper.append(lax.ppermute(upper[-1] if upper else x, axis, back))]
    all_to_all x2, starting transfers between devices: 20 us -> 24.9 us  [sum_at_owner(): pieces = lax.all_to_all(in_blocks(array, dim, size), axis, 0, 0, tiled=True)]
    all_to_all x2, waiting for transfers between devices: 25.9 us -> 22.5 us  [sum_at_owner(): pieces = lax.all_to_all(in_blocks(array, dim, size), axis, 0, 0, tiled=True)]
  transfers between devices with their start and end apart: 7 -> 22, of which waited for: 4 -> 16; matrix products, arithmetic and copies ran while one was open for 14% -> 13% of each run, Pallas kernels for 0% -> 0%
where the time goes in v1:
time: 301 us; the launch traced here: 300 us
  blocking collectives  133 us (44%)
  starting transfers between devices  75.1 us (25%)
  waiting for transfers between devices  74.8 us (25%)
  local copies, waits for them, and re-layouts  8.23 us (3%)
  other arithmetic  4.08 us (1%)
  matrix products  3.45 us (1%)
    ppermute x8, waiting for transfers between devices, ring_gather(): lower.append(lax.ppermute(lower[-1] if lower else x, axis, pairs))  42.5 us
    unnamed x1, blocking collectives  32.2 us
    all_to_all x1, blocking collectives, sum_at_owner(): pieces = lax.all_to_all(in_blocks(array, dim, size), axis, 0, 0, tiled=True)  31.3 us
    all_gather x1, blocking collectives, per_device(): lax.all_gather(hidden, 'kv', axis=0, tiled=True)  28.5 us
    all_gather x1, blocking collectives, per_device(): lax.all_gather(mixed, 'kv', axis=0, tiled=True)  25.4 us
    all_to_all x2, starting transfers between devices, sum_at_owner(): pieces = lax.all_to_all(in_blocks(array, dim, size), axis, 0, 0, tiled=True)  24.9 us
    ppermute x7, starting transfers between devices, ring_gather(): upper.append(lax.ppermute(upper[-1] if upper else x, axis, back))  24.8 us
    all_to_all x2, waiting for transfers between devices, sum_at_owner(): pieces = lax.all_to_all(in_blocks(array, dim, size), axis, 0, 0, tiled=True)  22.5 us
  transfers between devices with their start and end apart: 22, of which 16 were waited for; matrix products, arithmetic and copies ran while one was open for 13% of the time, Pallas kernels for 0%

profile of v1, /device:TPU:65, one launch (start us, length us, event | category | flops | bytes accessed | tf_op | source)
XLA Modules:
  0.0 300.0 jit_solution(17007136408794196316)
XLA Ops:
  0.6 2.7 collective-permute-start
  3.3 39.7 %collective-permute-done = bf16[320,16]{0,1:T(8,128)(2,1)S(1)} collective-permute-done((bf16[320,16]{0,1:T(8,128)(2,1)}, bf16[320,16]{0,1:T(8,128)(2,1)S(1)}, u32[]{:S(2)}, u32[]{:S(2)}) %collective-permute-start) | collective-permute-done | bytes 10272 | tf_op jit(solution)/shard_map/ppermute | solution.py:24
  43.0 3.6 %collective-permute-start.8 = (bf16[320,16]{0,1:T(8,128)(2,1)}, bf16[320,16]{0,1:T(8,128)(2,1)S(1)}, u32[]{:S(2)}, u32[]{:S(2)}) collective-permute-start(bf16[320,16]{0,1:T(8,128)(2,1)} %param.14), channel_id=1, source_target_pairs={{1,0},{2,1},{3,2},{4,3},{5,4},{6,5},{7,6},{8,7},{9,8},{10,9},{11,1... | collective-permute-start | bytes 30728 | tf_op jit(solution)/shard_map/ppermute | solution.py:26
  46.7 0.7 collective-permute-done.1
  47.3 0.4 collective-permute-done.8
  47.7 3.5 %collective-permute-start.9 = (bf16[320,16]{0,1:T(8,128)(2,1)S(1)}, bf16[320,16]{0,1:T(8,128)(2,1)S(1)}, u32[]{:S(2)}, u32[]{:S(2)}) collective-permute-start(bf16[320,16]{0,1:T(8,128)(2,1)S(1)} %collective-permute-done.8), channel_id=1, source_target_pairs={{1,0},{2,1},{3,2},{4,3},{5,4},{6,5},{7,6},{8,7},{9,8},{10,9},{11,1... | collective-permute-start | bytes 30728 | tf_op jit(solution)/shard_map/ppermute | solution.py:26
  51.2 0.4 collective-permute-done.2
  51.7 0.4 collective-permute-done.9
  52.1 3.5 %collective-permute-start.10 = (bf16[320,16]{0,1:T(8,128)(2,1)S(1)}, bf16[320,16]{0,1:T(8,128)(2,1)S(1)}, u32[]{:S(2)}, u32[]{:S(2)}) collective-permute-start(bf16[320,16]{0,1:T(8,128)(2,1)S(1)} %collective-permute-done.9), channel_id=1, source_target_pairs={{1,0},{2,1},{3,2},{4,3},{5,4},{6,5},{7,6},{8,7},{9,8},{10,9},{11,1... | collective-permute-start | bytes 30728 | tf_op jit(solution)/shard_map/ppermute | solution.py:26
  55.6 0.4 collective-permute-done.3
  56.0 0.4 collective-permute-done.10
  56.4 3.5 %collective-permute-start.11 = (bf16[320,16]{0,1:T(8,128)(2,1)S(1)}, bf16[320,16]{0,1:T(8,128)(2,1)S(1)}, u32[]{:S(2)}, u32[]{:S(2)}) collective-permute-start(bf16[320,16]{0,1:T(8,128)(2,1)S(1)} %collective-permute-done.10), channel_id=1, source_target_pairs={{1,0},{2,1},{3,2},{4,3},{5,4},{6,5},{7,6},{8,7},{9,8},{10,9},{11,1... | collective-permute-start | bytes 30728 | tf_op jit(solution)/shard_map/ppermute | solution.py:26
  59.9 0.4 collective-permute-done.4
  60.3 0.4 collective-permute-done.11
  60.7 3.5 %collective-permute-start.12 = (bf16[320,16]{0,1:T(8,128)(2,1)S(1)}, bf16[320,16]{0,1:T(8,128)(2,1)S(1)}, u32[]{:S(2)}, u32[]{:S(2)}) collective-permute-start(bf16[320,16]{0,1:T(8,128)(2,1)S(1)} %collective-permute-done.11), channel_id=1, source_target_pairs={{1,0},{2,1},{3,2},{4,3},{5,4},{6,5},{7,6},{8,7},{9,8},{10,9},{11,1... | collective-permute-start | bytes 30728 | tf_op jit(solution)/shard_map/ppermute | solution.py:26
  64.2 0.4 collective-permute-done.5
  64.7 0.4 collective-permute-done.12
  65.1 3.5 %collective-permute-start.13 = (bf16[320,16]{0,1:T(8,128)(2,1)S(1)}, bf16[320,16]{0,1:T(8,128)(2,1)S(1)}, u32[]{:S(2)}, u32[]{:S(2)}) collective-permute-start(bf16[320,16]{0,1:T(8,128)(2,1)S(1)} %collective-permute-done.12), channel_id=1, source_target_pairs={{1,0},{2,1},{3,2},{4,3},{5,4},{6,5},{7,6},{8,7},{9,8},{10,9},{11,1... | collective-permute-start | bytes 30728 | tf_op jit(solution)/shard_map/ppermute | solution.py:26
  68.6 0.4 collective-permute-done.6
  69.0 0.7 convert_element_type.89
  69.7 3.7 %collective-permute-start.14 = (bf16[320,16]{0,1:T(8,128)(2,1)S(1)}, bf16[320,16]{0,1:T(8,128)(2,1)S(1)}, u32[]{:S(2)}, u32[]{:S(2)}) collective-permute-start(bf16[320,16]{0,1:T(8,128)(2,1)S(1)} %collective-permute-done.13), channel_id=1, source_target_pairs={{1,0},{2,1},{3,2},{4,3},{5,4},{6,5},{7,6},{8,7},{9,8},{10,9},{11,1... | collective-permute-start | bytes 30728 | tf_op jit(solution)/shard_map/ppermute | solution.py:26
  73.4 0.7 constant_dynamic-update-slice_fusion.7
  74.2 0.6 gather_fusion
  74.9 0.6 broadcast_in_dim.4
  75.5 3.9 %all-to-all-start.1 = ((f32[16,1,320]{2,1,0:T(1,128)}), f32[16,1,320]{2,1,0:T(1,128)S(1)}, u32[]{:S(2)}, u32[]{:S(2)}) async-start(f32[16,1,320]{2,1,0:T(1,128)} %broadcast_in_dim.4), calls=%async_computation.1 | async-start | bytes 49152 | tf_op jit(solution)/shard_map/all_to_all | solution.py:35
  79.4 1.3 reshape.263
  80.8 1.1 copy.43
  82.0 0.2 convolution_convert_fusion.6
  82.2 0.2 convolution_convert_fusion.5
  82.5 0.2 convolution_convert_fusion.4
  82.8 0.2 convolution_convert_fusion.7
  83.0 0.8 pad_maximum_fusion.1
  83.8 6.7 %all-to-all-done.1 = f32[16,1,320]{2,1,0:T(1,128)S(1)} async-done(((f32[16,1,320]{2,1,0:T(1,128)}), f32[16,1,320]{2,1,0:T(1,128)S(1)}, u32[]{:S(2)}, u32[]{:S(2)}) %all-to-all-start.1) | async-done | bytes 20512 | tf_op jit(solution)/shard_map/all_to_all | solution.py:35
  90.5 4.6 %all-to-all-start = ((bf16[16,20,512]{2,1,0:T(8,128)(2,1)}), bf16[16,20,512]{2,1,0:T(8,128)(2,1)S(1)}, u32[]{:S(2)}, u32[]{:S(2)}) async-start(bf16[16,20,512]{2,1,0:T(8,128)(2,1)} %pad_maximum_fusion.1), calls=%async_computation | async-start | bytes 786432 | tf_op jit(solution)/shard_map/all_to_all | solution.py:51
  95.4 14.2 %all-to-all-done = bf16[16,20,512]{2,1,0:T(8,128)(2,1)S(1)} async-done(((bf16[16,20,512]{2,1,0:T(8,128)(2,1)}), bf16[16,20,512]{2,1,0:T(8,128)(2,1)S(1)}, u32[]{:S(2)}, u32[]{:S(2)}) %all-to-all-start) | async-done | bytes 327712 | tf_op jit(solution)/shard_map/all_to_all | solution.py:51
  109.8 0.1 fusion.28
  110.1 0.4 multiply_add_fusion
  110.5 1.2 fusion.1
  111.7 0.1 bitcast_reduce_fusion
  111.9 0.2 multiply_reduce_fusion
  112.1 25.4 %all-gather = bf16[16,20,128]{2,1,0:T(8,128)(2,1)S(1)} all-gather(bf16[1,20,128]{2,1,0:T(8,128)(2,1)S(1)} %fusion.35), channel_id=1, replica_groups=mesh['grp'=2,'kv'=16,'tp'=16] {'kv'}, dimensions={0}, use_global_device_ids=true | all-gather | bytes 87040 | tf_op jit(solution)/shard_map/all_gather | solution.py:147
  137.6 0.2 convolution_convert_fusion.3
  137.8 0.8 copy.49
  138.6 20.3 %all-to-all-start.2 = ((bf16[16,320,16]{1,2,0:T(8,128)(2,1)}), bf16[16,320,16]{1,2,0:T(8,128)(2,1)S(1)}, u32[]{:S(2)}, u32[]{:S(2)}) async-start(bf16[16,320,16]{1,2,0:T(8,128)(2,1)} %bitcast.32), calls=%async_computation.2 | async-start | bytes 393216 | tf_op jit(solution)/shard_map/all_to_all | solution.py:51
  158.9 1.3 dynamic-slice.4
  160.8 8.3 %all-to-all-done.2 = bf16[16,320,16]{1,2,0:T(8,128)(2,1)S(1)} async-done(((bf16[16,320,16]{1,2,0:T(8,128)(2,1)}), bf16[16,320,16]{1,2,0:T(8,128)(2,1)S(1)}, u32[]{:S(2)}, u32[]{:S(2)}) %all-to-all-start.2) | async-done | bytes 163872 | tf_op jit(solution)/shard_map/all_to_all | solution.py:51
  169.1 15.1 %all_gather.10 = bf16[320,256]{0,1:T(8,128)(2,1)S(1)} all-gather(bf16[320,16]{0,1:T(8,128)(2,1)S(1)} %add_convert_fusion.1), channel_id=1, replica_groups=mesh['grp'=2,'kv'=16,'tp'=16] {'tp'}, dimensions={1}, use_global_device_ids=true | all-gather | bytes 174080 | tf_op jit(solution)/shard_map/all_gather | solution.py:152
  184.3 0.6 broadcast_in_dim.5
  184.9 7.6 %all-to-all-start.3 = ((f32[16,1,320]{2,1,0:T(1,128)}), f32[16,1,320]{2,1,0:T(1,128)S(1)}, u32[]{:S(2)}, u32[]{:S(2)}) async-start(f32[16,1,320]{2,1,0:T(1,128)} %broadcast_in_dim.5), calls=%async_computation.3 | async-start | bytes 49152 | tf_op jit(solution)/shard_map/all_to_all | solution.py:35
  192.5 0.4 convolution_convert_fusion
  193.0 0.4 convolution_convert_fusion.1
  193.5 32.2 %fusion = bf16[24,1792]{1,0:T(8,128)(2,1)S(1)} fusion(bf16[320,1792]{1,0:T(8,128)(2,1)S(1)} %pad_maximum_fusion), kind=kCustom, calls=%all-reduce-scatter | all-reduce-scatter fusion | flops 688129 | bytes 1234944
  225.7 2.7 collective-permute-start.16
  228.4 2.9 collective-permute-start.15
  231.4 5.5 %collective-permute-start.17 = (bf16[12,1792]{1,0:T(8,128)(2,1)S(1)}, bf16[12,1792]{1,0:T(8,128)(2,1)S(1)}, u32[]{:S(2)}, u32[]{:S(2)}) collective-permute-start(bf16[12,1792]{1,0:T(8,128)(2,1)S(1)} %slice.52), channel_id=1, source_target_pairs={{0,48},{16,64},{32,80},{48,96},{64,112},{80,128},{96,144},{112,160... | collective-permute-start | bytes 129032
  237.0 1.1 collective-permute-done.17
  238.1 0.6 concatenate.28
  238.8 0.1 fusion.18
  238.9 28.5 %all-gather.1 = bf16[16,20,896]{2,1,0:T(8,128)(2,1)S(1)} all-gather(bf16[1,20,896]{2,1,0:T(8,128)(2,1)S(1)} %fusion.18), channel_id=1, replica_groups=mesh['grp'=2,'kv'=16,'tp'=16] {'kv'}, dimensions={0}, use_global_device_ids=true | all-gather | bytes 609280 | tf_op jit(solution)/shard_map/all_gather | solution.py:181
  267.4 0.1 reshape.279
  267.6 0.3 convolution_convert_fusion.2
  267.9 0.2 copy.51
  268.1 31.3 %all_to_all.27 = bf16[16,320,16]{1,2,0:T(8,128)(2,1)S(1)} all-to-all(bf16[16,320,16]{1,2,0:T(8,128)(2,1)S(1)} %bitcast.93), channel_id=1, replica_groups=mesh['grp'=2,'kv'=16,'tp'=16] {'tp'}, dimensions={0} | all-to-all | bytes 327680 | tf_op jit(solution)/shard_map/all_to_all | solution.py:51
  299.4 0.6 add_convert_fusion
  (85 shorter events, 1.4 us)
Async XLA Ops:
  0.6 191.9 %copy-start = (bf16[256,896]{1,0:T(8,128)(2,1)S(1)}, bf16[256,896]{1,0:T(8,128)(2,1)}, u32[]{:S(2)}) copy-start(bf16[256,896]{1,0:T(8,128)(2,1)} %param.26) | copy-start | bytes 1376260
  0.6 42.4 %collective-permute-start = (bf16[320,16]{0,1:T(8,128)(2,1)}, bf16[320,16]{0,1:T(8,128)(2,1)S(1)}, u32[]{:S(2)}, u32[]{:S(2)}) collective-permute-start(bf16[320,16]{0,1:T(8,128)(2,1)} %param.14), channel_id=1, source_target_pairs={{0,1},{1,2},{2,3},{3,4},{4,5},{5,6},{6,7},{7,8},{8,9},{9,10},{10,1... | collective-permute-start | bytes 30728 | tf_op jit(solution)/shard_map/ppermute | solution.py:24
  43.0 4.3 %collective-permute-start.1 = (bf16[320,16]{0,1:T(8,128)(2,1)S(1)}, bf16[320,16]{0,1:T(8,128)(2,1)S(1)}, u32[]{:S(2)}, u32[]{:S(2)}) collective-permute-start(bf16[320,16]{0,1:T(8,128)(2,1)S(1)} %collective-permute-done), channel_id=1, source_target_pairs={{0,1},{1,2},{2,3},{3,4},{4,5},{5,6},{6,7},{7,8},{8,9},{9,10},{10,1... | collective-permute-start | bytes 30728 | tf_op jit(solution)/shard_map/ppermute | solution.py:24
  43.0 4.7 %collective-permute-start.8 = (bf16[320,16]{0,1:T(8,128)(2,1)}, bf16[320,16]{0,1:T(8,128)(2,1)S(1)}, u32[]{:S(2)}, u32[]{:S(2)}) collective-permute-start(bf16[320,16]{0,1:T(8,128)(2,1)} %param.14), channel_id=1, source_target_pairs={{1,0},{2,1},{3,2},{4,3},{5,4},{6,5},{7,6},{8,7},{9,8},{10,9},{11,1... | collective-permute-start | bytes 30728 | tf_op jit(solution)/shard_map/ppermute | solution.py:26
  47.3 4.3 %collective-permute-start.2 = (bf16[320,16]{0,1:T(8,128)(2,1)S(1)}, bf16[320,16]{0,1:T(8,128)(2,1)S(1)}, u32[]{:S(2)}, u32[]{:S(2)}) collective-permute-start(bf16[320,16]{0,1:T(8,128)(2,1)S(1)} %collective-permute-done.1), channel_id=1, source_target_pairs={{0,1},{1,2},{2,3},{3,4},{4,5},{5,6},{6,7},{7,8},{8,9},{9,10},{10,1... | collective-permute-start | bytes 30728 | tf_op jit(solution)/shard_map/ppermute | solution.py:24
  47.7 4.4 %collective-permute-start.9 = (bf16[320,16]{0,1:T(8,128)(2,1)S(1)}, bf16[320,16]{0,1:T(8,128)(2,1)S(1)}, u32[]{:S(2)}, u32[]{:S(2)}) collective-permute-start(bf16[320,16]{0,1:T(8,128)(2,1)S(1)} %collective-permute-done.8), channel_id=1, source_target_pairs={{1,0},{2,1},{3,2},{4,3},{5,4},{6,5},{7,6},{8,7},{9,8},{10,9},{11,1... | collective-permute-start | bytes 30728 | tf_op jit(solution)/shard_map/ppermute | solution.py:26
  51.7 4.3 %collective-permute-start.3 = (bf16[320,16]{0,1:T(8,128)(2,1)S(1)}, bf16[320,16]{0,1:T(8,128)(2,1)S(1)}, u32[]{:S(2)}, u32[]{:S(2)}) collective-permute-start(bf16[320,16]{0,1:T(8,128)(2,1)S(1)} %collective-permute-done.2), channel_id=1, source_target_pairs={{0,1},{1,2},{2,3},{3,4},{4,5},{5,6},{6,7},{7,8},{8,9},{9,10},{10,1... | collective-permute-start | bytes 30728 | tf_op jit(solution)/shard_map/ppermute | solution.py:24
  52.1 4.3 %collective-permute-start.10 = (bf16[320,16]{0,1:T(8,128)(2,1)S(1)}, bf16[320,16]{0,1:T(8,128)(2,1)S(1)}, u32[]{:S(2)}, u32[]{:S(2)}) collective-permute-start(bf16[320,16]{0,1:T(8,128)(2,1)S(1)} %collective-permute-done.9), channel_id=1, source_target_pairs={{1,0},{2,1},{3,2},{4,3},{5,4},{6,5},{7,6},{8,7},{9,8},{10,9},{11,1... | collective-permute-start | bytes 30728 | tf_op jit(solution)/shard_map/ppermute | solution.py:26
  56.0 4.3 %collective-permute-start.4 = (bf16[320,16]{0,1:T(8,128)(2,1)S(1)}, bf16[320,16]{0,1:T(8,128)(2,1)S(1)}, u32[]{:S(2)}, u32[]{:S(2)}) collective-permute-start(bf16[320,16]{0,1:T(8,128)(2,1)S(1)} %collective-permute-done.3), channel_id=1, source_target_pairs={{0,1},{1,2},{2,3},{3,4},{4,5},{5,6},{6,7},{7,8},{8,9},{9,10},{10,1... | collective-permute-start | bytes 30728 | tf_op jit(solution)/shard_map/ppermute | solution.py:24
  56.4 4.3 %collective-permute-start.11 = (bf16[320,16]{0,1:T(8,128)(2,1)S(1)}, bf16[320,16]{0,1:T(8,128)(2,1)S(1)}, u32[]{:S(2)}, u32[]{:S(2)}) collective-permute-start(bf16[320,16]{0,1:T(8,128)(2,1)S(1)} %collective-permute-done.10), channel_id=1, source_target_pairs={{1,0},{2,1},{3,2},{4,3},{5,4},{6,5},{7,6},{8,7},{9,8},{10,9},{11,1... | collective-permute-start | bytes 30728 | tf_op jit(solution)/shard_map/ppermute | solution.py:26
  60.3 4.3 %collective-permute-start.5 = (bf16[320,16]{0,1:T(8,128)(2,1)S(1)}, bf16[320,16]{0,1:T(8,128)(2,1)S(1)}, u32[]{:S(2)}, u32[]{:S(2)}) collective-permute-start(bf16[320,16]{0,1:T(8,128)(2,1)S(1)} %collective-permute-done.4), channel_id=1, source_target_pairs={{0,1},{1,2},{2,3},{3,4},{4,5},{5,6},{6,7},{7,8},{8,9},{9,10},{10,1... | collective-permute-start | bytes 30728 | tf_op jit(solution)/shard_map/ppermute | solution.py:24
  60.7 4.3 %collective-permute-start.12 = (bf16[320,16]{0,1:T(8,128)(2,1)S(1)}, bf16[320,16]{0,1:T(8,128)(2,1)S(1)}, u32[]{:S(2)}, u32[]{:S(2)}) collective-permute-start(bf16[320,16]{0,1:T(8,128)(2,1)S(1)} %collective-permute-done.11), channel_id=1, source_target_pairs={{1,0},{2,1},{3,2},{4,3},{5,4},{6,5},{7,6},{8,7},{9,8},{10,9},{11,1... | collective-permute-start | bytes 30728 | tf_op jit(solution)/shard_map/ppermute | solution.py:26
  64.7 4.3 %collective-permute-start.6 = (bf16[320,16]{0,1:T(8,128)(2,1)S(1)}, bf16[320,16]{0,1:T(8,128)(2,1)S(1)}, u32[]{:S(2)}, u32[]{:S(2)}) collective-permute-start(bf16[320,16]{0,1:T(8,128)(2,1)S(1)} %collective-permute-done.5), channel_id=1, source_target_pairs={{0,1},{1,2},{2,3},{3,4},{4,5},{5,6},{6,7},{7,8},{8,9},{9,10},{10,1... | collective-permute-start | bytes 30728 | tf_op jit(solution)/shard_map/ppermute | solution.py:24
  65.1 4.6 %collective-permute-start.13 = (bf16[320,16]{0,1:T(8,128)(2,1)S(1)}, bf16[320,16]{0,1:T(8,128)(2,1)S(1)}, u32[]{:S(2)}, u32[]{:S(2)}) collective-permute-start(bf16[320,16]{0,1:T(8,128)(2,1)S(1)} %collective-permute-done.12), channel_id=1, source_target_pairs={{1,0},{2,1},{3,2},{4,3},{5,4},{6,5},{7,6},{8,7},{9,8},{10,9},{11,1... | collective-permute-start | bytes 30728 | tf_op jit(solution)/shard_map/ppermute | solution.py:26
  69.0 4.3 %collective-permute-start.7 = (bf16[320,16]{0,1:T(8,128)(2,1)S(1)}, bf16[320,16]{0,1:T(8,128)(2,1)S(1)}, u32[]{:S(2)}, u32[]{:S(2)}) collective-permute-start(bf16[320,16]{0,1:T(8,128)(2,1)S(1)} %collective-permute-done.6), channel_id=1, source_target_pairs={{0,1},{1,2},{2,3},{3,4},{4,5},{5,6},{6,7},{7,8},{8,9},{9,10},{10,1... | collective-permute-start | bytes 30728 | tf_op jit(solution)/shard_map/ppermute | solution.py:24
  69.7 4.5 %collective-permute-start.14 = (bf16[320,16]{0,1:T(8,128)(2,1)S(1)}, bf16[320,16]{0,1:T(8,128)(2,1)S(1)}, u32[]{:S(2)}, u32[]{:S(2)}) collective-permute-start(bf16[320,16]{0,1:T(8,128)(2,1)S(1)} %collective-permute-done.13), channel_id=1, source_target_pairs={{1,0},{2,1},{3,2},{4,3},{5,4},{6,5},{7,6},{8,7},{9,8},{10,9},{11,1... | collective-permute-start | bytes 30728 | tf_op jit(solution)/shard_map/ppermute | solution.py:26
  75.5 15.0 %all-to-all-start.1 = ((f32[16,1,320]{2,1,0:T(1,128)}), f32[16,1,320]{2,1,0:T(1,128)S(1)}, u32[]{:S(2)}, u32[]{:S(2)}) async-start(f32[16,1,320]{2,1,0:T(1,128)} %broadcast_in_dim.4), calls=%async_computation.1 | async-start | bytes 49152 | tf_op jit(solution)/shard_map/all_to_all | solution.py:35
  80.7 1.2 copy-start.6
  80.7 1.5 copy-start.7
  80.8 1.7 copy-start.8
  81.9 0.8 copy-start.9
  82.2 13.0 %copy-start.11 = (s32[20]{0:T(128)S(1)}, s32[20]{0:T(128)}, u32[]{:S(2)}) copy-start(s32[20]{0:T(128)} %param.15) | copy-start | bytes 244
  82.2 13.0 %copy-start.12 = (bf16[128]{0:T(256)(128)(2,1)S(1)}, bf16[128]{0:T(256)(128)(2,1)}, u32[]{:S(2)}) copy-start(bf16[128]{0:T(256)(128)(2,1)} %param.22) | copy-start | bytes 772
  82.8 27.3 %copy-start.2 = (f32[20,1,128,128]{3,2,1,0:T(8,128)S(1)}, f32[20,1,128,128]{3,2,1,0:T(8,128)}, u32[]{:S(2)}) copy-start(f32[20,1,128,128]{3,2,1,0:T(8,128)} %param.16) | copy-start | bytes 3932164
  90.5 19.1 %all-to-all-start = ((bf16[16,20,512]{2,1,0:T(8,128)(2,1)}), bf16[16,20,512]{2,1,0:T(8,128)(2,1)S(1)}, u32[]{:S(2)}, u32[]{:S(2)}) async-start(bf16[16,20,512]{2,1,0:T(8,128)(2,1)} %pad_maximum_fusion.1), calls=%async_computation | async-start | bytes 786432 | tf_op jit(solution)/shard_map/all_to_all | solution.py:51
  110.5 28.1 %copy-start.1 = (f32[20,1,128,128]{3,2,1,0:T(8,128)}, f32[20,1,128,128]{3,2,1,0:T(8,128)S(1)}, u32[]{:S(2)}) copy-start(f32[20,1,128,128]{3,2,1,0:T(8,128)S(1)} %multiply_add_fusion) | copy-start | bytes 3932164
  110.5 27.1 %copy-start.5 = (bf16[128,256]{1,0:T(8,128)(2,1)S(1)}, bf16[128,256]{1,0:T(8,128)(2,1)}, u32[]{:S(2)}) copy-start(bf16[128,256]{1,0:T(8,128)(2,1)} %param.23) | copy-start | bytes 196612
  110.5 48.4 %copy-start.13 = (bf16[256]{0:T(256)(128)(2,1)S(1)}, bf16[256]{0:T(256)(128)(2,1)}, u32[]{:S(2)}) copy-start(bf16[256]{0:T(256)(128)(2,1)} %param.24) | copy-start | bytes 1540
  110.5 58.6 %copy-start.10 = (bf16[320,16]{0,1:T(8,128)(2,1)S(1)}, bf16[320,16]{0,1:T(8,128)(2,1)}, u32[]{:S(2)}) copy-start(bf16[320,16]{0,1:T(8,128)(2,1)} %param.14) | copy-start | bytes 30724
  137.8 55.2 %copy-start.3 = (bf16[256,896]{1,0:T(8,128)(2,1)S(1)}, bf16[256,896]{1,0:T(8,128)(2,1)}, u32[]{:S(2)}) copy-start(bf16[256,896]{1,0:T(8,128)(2,1)} %param.25) | copy-start | bytes 1376260
  138.6 30.5 %all-to-all-start.2 = ((bf16[16,320,16]{1,2,0:T(8,128)(2,1)}), bf16[16,320,16]{1,2,0:T(8,128)(2,1)S(1)}, u32[]{:S(2)}, u32[]{:S(2)}) async-start(bf16[16,320,16]{1,2,0:T(8,128)(2,1)} %bitcast.32), calls=%async_computation.2 | async-start | bytes 393216 | tf_op jit(solution)/shard_map/all_to_all | solution.py:51
  184.9 52.0 %all-to-all-start.3 = ((f32[16,1,320]{2,1,0:T(1,128)}), f32[16,1,320]{2,1,0:T(1,128)S(1)}, u32[]{:S(2)}, u32[]{:S(2)}) async-start(f32[16,1,320]{2,1,0:T(1,128)} %broadcast_in_dim.5), calls=%async_computation.3 | async-start | bytes 49152 | tf_op jit(solution)/shard_map/all_to_all | solution.py:35
  225.7 12.4 %collective-permute-start.16 = (bf16[24,1792]{1,0:T(8,128)(2,1)S(1)}, bf16[24,1792]{1,0:T(8,128)(2,1)S(1)}, u32[]{:S(2)}, u32[]{:S(2)}) collective-permute-start(bf16[24,1792]{1,0:T(8,128)(2,1)S(1)} %fusion), channel_id=1, source_target_pairs={{0,32},{16,48},{32,64},{48,80},{64,96},{80,112},{96,128},{112,144}... | collective-permute-start | bytes 258056
  228.4 9.7 %collective-permute-start.15 = (bf16[24,1792]{1,0:T(8,128)(2,1)S(1)}, bf16[24,1792]{1,0:T(8,128)(2,1)S(1)}, u32[]{:S(2)}, u32[]{:S(2)}) collective-permute-start(bf16[24,1792]{1,0:T(8,128)(2,1)S(1)} %fusion), channel_id=1, source_target_pairs={{0,16},{16,32},{32,48},{48,64},{64,80},{80,96},{96,112},{112,128},... | collective-permute-start | bytes 258056
  231.4 6.8 %collective-permute-start.17 = (bf16[12,1792]{1,0:T(8,128)(2,1)S(1)}, bf16[12,1792]{1,0:T(8,128)(2,1)S(1)}, u32[]{:S(2)}, u32[]{:S(2)}) collective-permute-start(bf16[12,1792]{1,0:T(8,128)(2,1)S(1)} %slice.52), channel_id=1, source_target_pairs={{0,48},{16,64},{32,80},{48,96},{64,112},{80,128},{96,144},{112,160... | collective-permute-start | bytes 129032
  238.7 28.8 %copy-start.4 = (bf16[896,256]{1,0:T(8,128)(2,1)S(1)}, bf16[896,256]{1,0:T(8,128)(2,1)}, u32[]{:S(2)}) copy-start(bf16[896,256]{1,0:T(8,128)(2,1)} %param.27) | copy-start | bytes 1376260
